TPU v7x, 32 devices: a whole 2x2x4 slice. The times are simulated.
32 devices in a mesh: sp: 8 (over z, y), tp: 4 (over x, core).
Axes of the slice: x: 2, y: 2, z: 4, core: 2. Of those that a mesh axis runs over, the one named last changes fastest.
Arguments:
- residual_entry_input: bfloat16 [8192, 2048], P(('sp', 'tp')), may hold values from -6 to 6
- query_matrix_rows: bfloat16 [8192, 1024], P('sp', 'tp'), may hold values from -6 to 6
- key_matrix_rows: bfloat16 [8192, 1024], P('sp', 'tp'), may hold values from -6 to 6
- value_matrix_rows: bfloat16 [8192, 2048], P('sp', 'tp'), may hold values from -6 to 6
- output_gate_logits: bfloat16 [8192, 2048], P('sp', 'tp'), may hold values from -6 to 6
- input_gate_logits: float32 [8192, 8], P('sp', 'tp'), may hold values from -6 to 6
- forget_gate_logits: float32 [8192, 8], P('sp', 'tp'), may hold values from -8 to 31
- forget_decay_offset: float32 [8192, 8], P('sp', 'tp'), may hold values from -0.7 to 0
- head_norm_gain: float32 [8, 256], P('tp'), may hold values from 0.1 to 1.9
- cell_output_weight: bfloat16 [2048, 2048], P('tp'), may hold values from -0.125 to 0.125
- feedforward_norm_gain: float32 [2048], replicated, may hold values from 0.1 to 1.9
- gate_up_weight: bfloat16 [2048, 5632], P('sp', 'tp'), may hold values from -0.125 to 0.125
- value_up_weight: bfloat16 [2048, 5632], P('sp', 'tp'), may hold values from -0.125 to 0.125
- gate_filter_taps: float32 [3, 5632], P(None, 'tp'), may hold values from -3 to 3
- value_filter_taps: float32 [3, 5632], P(None, 'tp'), may hold values from -3 to 3
- down_projection_weight: bfloat16 [5632, 2048], P('tp', 'sp'), may hold values from -0.078125 to 0.078125
Outputs:
- result: bfloat16 [8192, 2048], P(('sp', 'tp'))
All inputs are finite; a program needn't handle non-finite values.
Results may differ from a plain program's by a relative error of at most 0.025.
Values may be sent and summed in bfloat16 or wider, within the bound.
No kernel may reach another device: no remote copies, remote signals or barrier semaphores. Data moves between devices by JAX's collectives and lax.ppermute only.
A program may use at most 128 MiB of HBM per device.

v0:
```python
import jax
import jax.numpy as jnp
from jax import lax
from jax.sharding import PartitionSpec as P

BLOCK = 128
eps = 1e-06
neg_large = -1e30


def carried_in(x, axis, combine, identity):
    count, position = (lax.axis_size(axis), lax.axis_index(axis))
    everything = jax.tree.map(
        lambda part, kind: lax.all_gather(part.astype(kind), axis),
        x,
        (jnp.bfloat16, jnp.bfloat16, jnp.bfloat16, jnp.bfloat16),
    )
    start = jax.tree.map(
        lambda part, zero: jnp.broadcast_to(jnp.asarray(zero, part.dtype), part.shape), x, identity
    )

    def lap(k, before):
        reached = k < position
        new = combine(
            before, jax.tree.map(lambda part, own: part[k].astype(own.dtype), everything, x)
        )
        return jax.tree.map(lambda a, b: jnp.where(reached, a, b), new, before)

    return lax.fori_loop(0, count, lap, start)


def shifted(x, axis, by):
    count = lax.axis_size(axis)
    pairs = [(i, i + by) for i in range(count) if 0 <= i + by < count]
    return lax.ppermute(x, axis, pairs)


def gate_log_values(input_gate_logits, forget_gate_logits, forget_decay_offset):
    input_log_value = 15.0 * jnp.tanh(input_gate_logits / 15.0)
    forget_log_sigmoid = (
        jax.nn.log_sigmoid(15.0 * jnp.tanh(forget_gate_logits / 15.0)) + forget_decay_offset
    )
    return (input_log_value, forget_log_sigmoid)


def combine_states(earlier, later):
    total_one, memory_one, normer_one, running_one = earlier
    total_two, memory_two, normer_two, running_two = later
    joined = jnp.maximum(total_two + running_one, running_two)
    weight_one = jnp.exp(total_two + running_one - joined)
    weight_two = jnp.exp(running_two - joined)
    memory = weight_one[:, None, None] * memory_one + weight_two[:, None, None] * memory_two
    normer = weight_one[:, None] * normer_one + weight_two[:, None] * normer_two
    return (total_one + total_two, memory, normer, joined)


def local_step(state_carry, inputs):
    memory, normer, running = state_carry
    query_block, key_block, value_block, input_block, forget_block = inputs
    length = query_block.shape[0]
    highest = lax.Precision.HIGHEST
    query_scale = query_block.shape[2] ** (-0.5)
    causal = jnp.tril(jnp.ones((length, length), dtype=bool))[:, :, None]
    cumulative = jnp.cumsum(forget_block, axis=0)
    logits = cumulative[:, None, :] - cumulative[None, :, :] + input_block[None, :, :]
    logits = jnp.where(causal, logits, -jnp.inf)
    carried = cumulative + running[None, :]
    stable = jnp.maximum(carried, jnp.max(logits, axis=1))
    carry_weight = jnp.exp(carried - stable)
    raw = (
        jnp.einsum("thd,shd->tsh", query_block, key_block, preferred_element_type=jnp.float32)
        * query_scale
    )
    scores = raw * jnp.exp(logits - stable[:, None, :])
    scaled_query = query_block.astype(jnp.float32) * query_scale
    numerator = carry_weight[:, :, None] * jnp.einsum(
        "hvd,thd->thv", memory, scaled_query, precision=highest
    )
    numerator = numerator + jnp.einsum(
        "tsh,shv->thv", scores.astype(jnp.bfloat16), value_block, preferred_element_type=jnp.float32
    )
    denominator = carry_weight * jnp.einsum(
        "hd,thd->th", normer, scaled_query, precision=highest
    ) + jnp.sum(scores, axis=1)
    last_sum = cumulative[-1]
    weights_log = last_sum[None, :] - cumulative + input_block
    new_running = jnp.maximum(last_sum + running, jnp.max(weights_log, axis=0))
    decay_factor = jnp.exp(last_sum + running - new_running)
    weighted = (
        key_block.astype(jnp.float32) * jnp.exp(weights_log - new_running[None, :])[:, :, None]
    )
    memory = decay_factor[:, None, None] * memory + jnp.einsum(
        "shv,shd->hvd",
        value_block,
        weighted.astype(jnp.bfloat16),
        preferred_element_type=jnp.float32,
    )
    normer = decay_factor[:, None] * normer + jnp.sum(weighted, axis=0)
    return ((memory, normer, new_running), (numerator, denominator, stable))


def local(
    residual_entry_input,
    query_matrix_rows,
    key_matrix_rows,
    value_matrix_rows,
    output_gate_logits,
    input_gate_logits,
    forget_gate_logits,
    forget_decay_offset,
    head_norm_gain,
    cell_output_weight,
    feedforward_norm_gain,
    gate_up_weight,
    value_up_weight,
    gate_filter_taps,
    value_filter_taps,
    down_projection_weight,
):
    highest = lax.Precision.HIGHEST
    token_count = query_matrix_rows.shape[0]
    head_count = input_gate_logits.shape[1]
    key_width = query_matrix_rows.shape[1] // head_count
    value_width = value_matrix_rows.shape[1] // head_count
    query_scale = key_width ** (-0.5)
    queries_low = query_matrix_rows.reshape(token_count, head_count, key_width)
    keys_low = key_matrix_rows.reshape(token_count, head_count, key_width)
    values_low = value_matrix_rows.reshape(token_count, head_count, value_width)
    input_log_value, forget_log_sigmoid = gate_log_values(
        input_gate_logits, forget_gate_logits, forget_decay_offset
    )
    cumulative = jnp.cumsum(forget_log_sigmoid, axis=0)
    total_log = cumulative[-1]
    block_count = token_count // BLOCK

    def blocks(tensor):
        return tensor.reshape((block_count, BLOCK) + tensor.shape[1:])

    initial = (
        jnp.zeros((head_count, value_width, key_width), jnp.float32),
        jnp.zeros((head_count, key_width), jnp.float32),
        jnp.full((head_count,), neg_large, jnp.float32),
    )
    end_state, (numerator, denominator, stable) = lax.scan(
        local_step,
        initial,
        (
            blocks(queries_low),
            blocks(keys_low),
            blocks(values_low),
            blocks(input_log_value),
            blocks(forget_log_sigmoid),
        ),
    )
    end_memory, end_normer, end_running = end_state
    identity = (
        jnp.zeros((head_count,), jnp.float32),
        jnp.zeros((head_count, value_width, key_width), jnp.float32),
        jnp.zeros((head_count, key_width), jnp.float32),
        jnp.full((head_count,), neg_large, jnp.float32),
    )
    prefix = carried_in(
        (total_log, end_memory, end_normer, end_running), "sp", combine_states, identity
    )
    numerator = numerator.reshape(token_count, head_count, value_width)
    denominator = denominator.reshape(token_count, head_count)
    stable = stable.reshape(token_count, head_count)
    _, prior_memory, prior_normer, prior_running = prefix
    scaled_query = queries_low.astype(jnp.float32) * query_scale
    prior_log = cumulative + prior_running[None, :]
    top_log = jnp.maximum(stable, prior_log)
    local_weight = jnp.exp(stable - top_log)
    prior_weight = jnp.exp(prior_log - top_log)
    numerator = local_weight[:, :, None] * numerator + prior_weight[:, :, None] * jnp.einsum(
        "hvd,thd->thv", prior_memory, scaled_query, precision=highest
    )
    denominator = local_weight * denominator + prior_weight * jnp.einsum(
        "hd,thd->th", prior_normer, scaled_query, precision=highest
    )
    memory_out = numerator / jnp.maximum(jnp.abs(denominator), jnp.exp(-top_log))[:, :, None]
    normed = (
        memory_out
        * lax.rsqrt(jnp.mean(memory_out * memory_out, axis=-1, keepdims=True) + eps)
        * head_norm_gain[None, :, :]
    )
    gated_rows = (
        normed.reshape(token_count, head_count * value_width)
        * jax.nn.sigmoid(output_gate_logits.astype(jnp.float32))
    ).astype(jnp.bfloat16)
    whole_out = lax.all_gather(cell_output_weight, "tp", axis=0, tiled=True)
    own_rows = lax.all_to_all(gated_rows, "tp", split_axis=0, concat_axis=1, tiled=True)
    mixed_rows = jnp.dot(own_rows, whole_out, preferred_element_type=jnp.float32)
    stream_wide = residual_entry_input.astype(jnp.float32) + mixed_rows
    stream = stream_wide.astype(jnp.bfloat16)
    stream_wide = lax.optimization_barrier(stream).astype(jnp.float32)
    normed_rows = (
        stream_wide
        * lax.rsqrt(jnp.mean(stream_wide * stream_wide, axis=-1, keepdims=True) + eps)
        * feedforward_norm_gain[None, :]
    ).astype(jnp.bfloat16)
    group_rows = lax.all_gather(normed_rows, "tp", axis=0, tiled=True)
    earlier_rows = shifted(group_rows[-2:], "sp", 1)
    window = jnp.concatenate([earlier_rows, group_rows], axis=0)
    up_gate = jnp.dot(
        window,
        lax.all_gather(gate_up_weight, "sp", axis=0, tiled=True),
        preferred_element_type=jnp.float32,
    )
    up_value = jnp.dot(
        window,
        lax.all_gather(value_up_weight, "sp", axis=0, tiled=True),
        preferred_element_type=jnp.float32,
    )
    conv_g = (
        gate_filter_taps[0][None, :] * up_gate[:-2]
        + gate_filter_taps[1][None, :] * up_gate[1:-1]
        + gate_filter_taps[2][None, :] * up_gate[2:]
    )
    conv_v = (
        value_filter_taps[0][None, :] * up_value[:-2]
        + value_filter_taps[1][None, :] * up_value[1:-1]
        + value_filter_taps[2][None, :] * up_value[2:]
    )
    hidden = (jax.nn.silu(conv_g) * conv_v).astype(jnp.bfloat16)
    whole_down = lax.all_gather(down_projection_weight, "sp", axis=1, tiled=True)
    ffn_rows = lax.psum_scatter(
        jnp.dot(hidden, whole_down, preferred_element_type=jnp.float32).astype(jnp.bfloat16),
        "tp",
        scatter_dimension=0,
        tiled=True,
    ).astype(jnp.float32)
    return (stream_wide + ffn_rows).astype(jnp.bfloat16)


def solution(mesh):
    in_specs = (
        P(("sp", "tp"), None),
        P("sp", "tp"),
        P("sp", "tp"),
        P("sp", "tp"),
        P("sp", "tp"),
        P("sp", "tp"),
        P("sp", "tp"),
        P("sp", "tp"),
        P("tp", None),
        P("tp", None),
        P(),
        P("sp", "tp"),
        P("sp", "tp"),
        P(None, "tp"),
        P(None, "tp"),
        P("tp", "sp"),
    )
    out_specs = P(("sp", "tp"), None)
    return jax.shard_map(local, mesh=mesh, in_specs=in_specs, out_specs=out_specs, check_vma=False)
```

profile of v0, /device:TPU:0, one launch (start us, length us, event | category | flops | bytes accessed | tf_op | source)
XLA Modules:
  0.0 629.0 jit_solution(18224603662122398015)
XLA Ops:
  7.6 1.3 reshape.215
  9.9 2.0 reshape.216
  12.8 105.2 %while.39 = (s32[]{:T(128)}, f32[2,256,128]{2,1,0:T(8,128)S(1)}, f32[2,128]{1,0:T(2,128)S(1)}, f32[2]{0:T(128)S(1)}, f32[8,128,2,256]{1,0,3,2:T(8,128)}, /*index...) while((s32[]{:T(128)}, f32[2,256,128]{2,1,0:T(8,128)S(1)}, ...), condition=%wide.region_6.7_spmd.clone, body=%wide.region_0.6_spmd.clone.sunk | while | flops 144166400 | bytes 4685610 | solution.py:144
  13.6 1.0 constant_dynamic-slice_fusion.10
  17.3 8.2 %dynamic_update_slice.19 = f32[8,128,2,256]{1,0,3,2:T(8,128)} dynamic-update-slice(f32[8,128,2,256]{1,0,3,2:T(8,128)} %get-tuple-element.661, f32[1,128,2,256]{1,0,3,2:T(1,128)S(1)} %copy.248, s32[]{:T(128)} %get-tuple-element.657, s32[]{:T(128)} %constant.83.clone.1..sunk, s32[]{:T(128)} %constant.83.clone.1..sunk, s32[]{:T(128)} %constant.83.clone.1..sunk) | dynamic-update-slice | bytes 524292 | tf_op jit(solution)/shard_map/while/body/jit(dynamic_update_index_in_dim)/dynamic_update_slice | solution.py:144
  26.7 1.0 constant_dynamic-slice_fusion.10
  30.5 8.2 %dynamic_update_slice.19 = f32[8,128,2,256]{1,0,3,2:T(8,128)} dynamic-update-slice(f32[8,128,2,256]{1,0,3,2:T(8,128)} %get-tuple-element.661, f32[1,128,2,256]{1,0,3,2:T(1,128)S(1)} %copy.248, s32[]{:T(128)} %get-tuple-element.657, s32[]{:T(128)} %constant.83.clone.1..sunk, s32[]{:T(128)} %constant.83.clone.1..sunk, s32[]{:T(128)} %constant.83.clone.1..sunk) | dynamic-update-slice | bytes 524292 | tf_op jit(solution)/shard_map/while/body/jit(dynamic_update_index_in_dim)/dynamic_update_slice | solution.py:144
  43.7 8.2 %dynamic_update_slice.19 = f32[8,128,2,256]{1,0,3,2:T(8,128)} dynamic-update-slice(f32[8,128,2,256]{1,0,3,2:T(8,128)} %get-tuple-element.661, f32[1,128,2,256]{1,0,3,2:T(1,128)S(1)} %copy.248, s32[]{:T(128)} %get-tuple-element.657, s32[]{:T(128)} %constant.83.clone.1..sunk, s32[]{:T(128)} %constant.83.clone.1..sunk, s32[]{:T(128)} %constant.83.clone.1..sunk) | dynamic-update-slice | bytes 524292 | tf_op jit(solution)/shard_map/while/body/jit(dynamic_update_index_in_dim)/dynamic_update_slice | solution.py:144
  53.0 1.0 constant_dynamic-slice_fusion.10
  56.8 8.2 %dynamic_update_slice.19 = f32[8,128,2,256]{1,0,3,2:T(8,128)} dynamic-update-slice(f32[8,128,2,256]{1,0,3,2:T(8,128)} %get-tuple-element.661, f32[1,128,2,256]{1,0,3,2:T(1,128)S(1)} %copy.248, s32[]{:T(128)} %get-tuple-element.657, s32[]{:T(128)} %constant.83.clone.1..sunk, s32[]{:T(128)} %constant.83.clone.1..sunk, s32[]{:T(128)} %constant.83.clone.1..sunk) | dynamic-update-slice | bytes 524292 | tf_op jit(solution)/shard_map/while/body/jit(dynamic_update_index_in_dim)/dynamic_update_slice | solution.py:144
  66.2 1.0 constant_dynamic-slice_fusion.10
  70.0 8.2 %dynamic_update_slice.19 = f32[8,128,2,256]{1,0,3,2:T(8,128)} dynamic-update-slice(f32[8,128,2,256]{1,0,3,2:T(8,128)} %get-tuple-element.661, f32[1,128,2,256]{1,0,3,2:T(1,128)S(1)} %copy.248, s32[]{:T(128)} %get-tuple-element.657, s32[]{:T(128)} %constant.83.clone.1..sunk, s32[]{:T(128)} %constant.83.clone.1..sunk, s32[]{:T(128)} %constant.83.clone.1..sunk) | dynamic-update-slice | bytes 524292 | tf_op jit(solution)/shard_map/while/body/jit(dynamic_update_index_in_dim)/dynamic_update_slice | solution.py:144
  79.3 1.0 constant_dynamic-slice_fusion.10
  83.1 8.2 %dynamic_update_slice.19 = f32[8,128,2,256]{1,0,3,2:T(8,128)} dynamic-update-slice(f32[8,128,2,256]{1,0,3,2:T(8,128)} %get-tuple-element.661, f32[1,128,2,256]{1,0,3,2:T(1,128)S(1)} %copy.248, s32[]{:T(128)} %get-tuple-element.657, s32[]{:T(128)} %constant.83.clone.1..sunk, s32[]{:T(128)} %constant.83.clone.1..sunk, s32[]{:T(128)} %constant.83.clone.1..sunk) | dynamic-update-slice | bytes 524292 | tf_op jit(solution)/shard_map/while/body/jit(dynamic_update_index_in_dim)/dynamic_update_slice | solution.py:144
  96.3 8.2 %dynamic_update_slice.19 = f32[8,128,2,256]{1,0,3,2:T(8,128)} dynamic-update-slice(f32[8,128,2,256]{1,0,3,2:T(8,128)} %get-tuple-element.661, f32[1,128,2,256]{1,0,3,2:T(1,128)S(1)} %copy.248, s32[]{:T(128)} %get-tuple-element.657, s32[]{:T(128)} %constant.83.clone.1..sunk, s32[]{:T(128)} %constant.83.clone.1..sunk, s32[]{:T(128)} %constant.83.clone.1..sunk) | dynamic-update-slice | bytes 524292 | tf_op jit(solution)/shard_map/while/body/jit(dynamic_update_index_in_dim)/dynamic_update_slice | solution.py:144
  109.4 8.2 %dynamic_update_slice.19 = f32[8,128,2,256]{1,0,3,2:T(8,128)} dynamic-update-slice(f32[8,128,2,256]{1,0,3,2:T(8,128)} %get-tuple-element.661, f32[1,128,2,256]{1,0,3,2:T(1,128)S(1)} %copy.248, s32[]{:T(128)} %get-tuple-element.657, s32[]{:T(128)} %constant.83.clone.1..sunk, s32[]{:T(128)} %constant.83.clone.1..sunk, s32[]{:T(128)} %constant.83.clone.1..sunk) | dynamic-update-slice | bytes 524292 | tf_op jit(solution)/shard_map/while/body/jit(dynamic_update_index_in_dim)/dynamic_update_slice | solution.py:144
  122.2 22.3 %all-gather.3 = bf16[8,1,2]{2,1,0:T(2,128)(2,1)S(1)} all-gather(bf16[1,1,2]{2,1,0:T(2,128)(2,1)S(1)} %bitcast.273), channel_id=1, replica_groups=mesh['sp'=8,'tp'=4] {'sp'}, dimensions={0}, use_global_device_ids=true | all-gather | bytes 36 | tf_op jit(solution)/shard_map/all_gather | solution.py:14
  144.5 17.5 %all-reduce = bf16[16]{0:T(256)(128)(2,1)S(1)} all-reduce(bf16[16]{0:T(256)(128)(2,1)S(1)} %dynamic-update-slice), channel_id=2, replica_groups=mesh['sp'=8,'tp'=4] {'sp'}, use_global_device_ids=true, to_apply=%add | all-reduce | flops 16 | bytes 64
  162.2 1.2 copy.155
  163.5 1.3 copy.156
  164.8 1.7 reshape.187
  166.5 18.0 %all-gather.4 = bf16[8,2,128]{2,1,0:T(2,128)(2,1)S(1)} all-gather(bf16[1,2,128]{2,1,0:T(2,128)(2,1)S(1)} %convert_bitcast_fusion), channel_id=4, replica_groups=mesh['sp'=8,'tp'=4] {'sp'}, dimensions={0}, use_global_device_ids=true | all-gather | bytes 4608 | tf_op jit(solution)/shard_map/all_gather | solution.py:14
  184.5 10.5 %while.40 = (s32[]{:T(128)}, f32[2,256,128]{2,1,0:T(8,128)S(1)}, f32[2,128]{1,0:T(2,128)S(1)}, f32[2]{0:T(128)S(1)}, s32[]{:T(128)}, /*index=5*/bf16[8,2]{0,1:T(...) while((s32[]{:T(128)}, f32[2,256,128]{2,1,0:T(8,128)S(1)}, ...), condition=%wide.region_10.11_spmd.clone, body=%wide.region_9.10_spmd.clone.sunk | while | flops 394772 | bytes 658157 | solution.py:29
  184.7 1.0 fusion.107
  186.1 1.0 fusion.107
  187.4 1.0 fusion.107
  188.7 1.0 fusion.107
  190.0 1.0 fusion.107
  191.3 1.0 fusion.107
  192.6 1.0 fusion.107
  193.9 1.0 fusion.107
  195.1 1.0 fusion.52
  196.2 2.2 multiply_reduce_fusion
  198.7 1.9 copy.141
  200.6 2.5 multiply_convert_fusion
  203.1 26.9 %all_to_all.19 = bf16[4,256,512]{2,1,0:T(8,128)(2,1)S(1)} all-to-all(bf16[4,256,512]{2,1,0:T(8,128)(2,1)S(1)} %bitcast.262), channel_id=1, replica_groups=mesh['sp'=8,'tp'=4] {'tp'}, dimensions={0} | all-to-all | bytes 2097152 | tf_op jit(solution)/shard_map/all_to_all | solution.py:191
  230.5 5.7 fusion.45
  236.6 1.3 fusion.48
  239.9 33.9 %all-gather.14.cloned.1.call-done = bf16[1024,2048]{1,0:T(8,128)(2,1)} async-done(((bf16[256,2048]{1,0:T(8,128)(2,1)}), bf16[1024,2048]{1,0:T(8,128)(2,1)}) %all-gather.14.cloned.1.call-update) | async-done | bytes 4194320 | tf_op jit(solution)/shard_map/all_gather | solution.py:201
  274.6 3.4 collective-permute-start
  278.1 90.1 %all-gather.16.cloned.1.call-done = bf16[2048,1408]{1,0:T(8,128)(2,1)} async-done(((bf16[256,1408]{1,0:T(8,128)(2,1)}), bf16[2048,1408]{1,0:T(8,128)(2,1)}) %all-gather.16.cloned.1.call-update) | async-done | bytes 5767184 | tf_op jit(solution)/shard_map/all_gather | solution.py:206
  368.2 11.9 %fusion.44 = f32[1026,1408]{1,0:T(8,128)} fusion(bf16[2048,1408]{1,0:T(8,128)(2,1)} %all-gather.16.cloned.1.call-done, bf16[1024,2048]{1,0:T(8,128)(2,1)} %all-gather.14.cloned.1.call-done, bf16[2,2048]{1,0:T(2,128)(2,1)S(1)} %collective-permute-done), kind=kOutput, calls=%fused_computation.90 | convolution fusion | flops 5925519360 | bytes 15748096 | tf_op jit(solution)/shard_map/dot_general | solution.py:204
  380.1 80.6 %all-gather.18.cloned.1.call-done = bf16[2048,1408]{1,0:T(8,128)(2,1)} async-done(((bf16[256,1408]{1,0:T(8,128)(2,1)}), bf16[2048,1408]{1,0:T(8,128)(2,1)}) %all-gather.18.cloned.1.call-update) | async-done | bytes 5767184 | tf_op jit(solution)/shard_map/all_gather | solution.py:211
  460.7 11.9 %fusion.43 = f32[1026,1408]{1,0:T(8,128)} fusion(bf16[2048,1408]{1,0:T(8,128)(2,1)} %all-gather.18.cloned.1.call-done, bf16[1024,2048]{1,0:T(8,128)(2,1)} %all-gather.14.cloned.1.call-done, bf16[2,2048]{1,0:T(2,128)(2,1)S(1)} %collective-permute-done), kind=kOutput, calls=%fused_computation.89 | convolution fusion | flops 5925519360 | bytes 15748096 | tf_op jit(solution)/shard_map/dot_general | solution.py:209
  472.6 81.3 %all-gather.20.cloned.1.call-done = bf16[1408,2048]{1,0:T(8,128)(2,1)} async-done(((bf16[1408,256]{1,0:T(8,128)(2,1)}), bf16[1408,2048]{1,0:T(8,128)(2,1)}) %all-gather.20.cloned.1.call-update) | async-done | bytes 5767184 | tf_op jit(solution)/shard_map/all_gather | solution.py:225
  554.0 22.7 %convolution_convert_fusion = bf16[1024,2048]{1,0:T(8,128)(2,1)} fusion(bf16[1408,2048]{1,0:T(8,128)(2,1)} %all-gather.20.cloned.1.call-done, f32[1026,1408]{1,0:T(8,128)} %fusion.43, f32[1026,1408]{1,0:T(8,128)} %fusion.44, f32[1408]{0:T(1024)S(1)} %get-tuple-element.403, f32[1408]{0:T(1024)S(1)} %get-tuple-element.404, f32[1408]{0:T(1024)S(1)} %get-tuple-element.402, ...), kind=kOutput, calls=%fused_computation.85 | convolution fusion | flops 5930745856 | bytes 44598272 | tf_op jit(solution)/shard_map/dot_general | solution.py:227
  576.7 42.9 %reduce-scatter.2.cloned.1.call-done = bf16[256,2048]{1,0:T(8,128)(2,1)} async-done(((bf16[1024,2048]{1,0:T(8,128)(2,1)}), bf16[256,2048]{1,0:T(8,128)(2,1)}) %reduce-scatter.2.cloned.1.call-update) | async-done | bytes 1048592 | tf_op jit(solution)/shard_map/reduce_scatter | solution.py:226
  619.6 2.6 fusion.49
  (321 shorter events, 46.6 us)
Async XLA Ops:
  6.5 5.3 copy-start.1
  6.5 178.0 %all-gather.22.cloned.1.call-start = ((), (), s32[]{:S(2)}) async-start(), calls=%async_computation.8 | async-start | bytes 1179648 | tf_op jit(solution)/shard_map/all_gather | solution.py:14
  12.8 107.7 %copy-start.7 = (u32[32]{0:T(128)S(1)}, u32[32]{0:T(128)}, u32[]{:S(2)}) copy-start(u32[32]{0:T(128)} %constant.101) | copy-start | bytes 388
  118.7 111.8 %all-gather.12.cloned.1.call-start = ((), (), s32[]{:S(2)}) async-start(), calls=%async_computation.2 | async-start | bytes 10485760 | tf_op jit(solution)/shard_map/all_gather | solution.py:190
  119.4 154.4 %all-gather.14.cloned.1.call-start = ((), (), s32[]{:S(2)}) async-start(), calls=%async_computation.3 | async-start | bytes 5242880 | tf_op jit(solution)/shard_map/all_gather | solution.py:201
  163.5 31.6 %copy-start.2 = (bf16[1024,256]{1,0:T(8,128)(2,1)S(1)}, bf16[1024,256]{1,0:T(8,128)(2,1)}, u32[]{:S(2)}) copy-start(bf16[1024,256]{1,0:T(8,128)(2,1)} %param.21) | copy-start | bytes 1572868
  196.2 2.3 copy-start.6
  200.6 29.9 %copy-start = (bf16[256,2048]{1,0:T(8,128)(2,1)S(1)}, bf16[256,2048]{1,0:T(8,128)(2,1)}, u32[]{:S(2)}) copy-start(bf16[256,2048]{1,0:T(8,128)(2,1)} %param.20) | copy-start | bytes 3145732
  230.5 6.1 copy-start.5
  236.3 41.7 %copy-start.3 = (f32[3,1408]{1,0:T(4,128)S(1)}, f32[3,1408]{1,0:T(4,128)}, u32[]{:S(2)}) copy-start(f32[3,1408]{1,0:T(4,128)} %param.34) | copy-start | bytes 50692
  236.3 41.7 %copy-start.4 = (f32[3,1408]{1,0:T(4,128)S(1)}, f32[3,1408]{1,0:T(4,128)}, u32[]{:S(2)}) copy-start(f32[3,1408]{1,0:T(4,128)} %param.33) | copy-start | bytes 50692
  237.9 130.3 %all-gather.16.cloned.1.call-start = ((), (), s32[]{:S(2)}) async-start(), calls=%async_computation.4 | async-start | bytes 6488064 | tf_op jit(solution)/shard_map/all_gather | solution.py:206
  238.5 222.3 %all-gather.18.cloned.1.call-start = ((), (), s32[]{:S(2)}) async-start(), calls=%async_computation.5 | async-start | bytes 6488064 | tf_op jit(solution)/shard_map/all_gather | solution.py:211
  239.1 314.9 %all-gather.20.cloned.1.call-start = ((), (), s32[]{:S(2)}) async-start(), calls=%async_computation.6 | async-start | bytes 6488064 | tf_op jit(solution)/shard_map/all_gather | solution.py:225
  239.7 379.9 %reduce-scatter.2.cloned.1.call-start = ((), (), s32[]{:S(2)}) async-start(), calls=%async_computation.7 | async-start | bytes 5242880 | tf_op jit(solution)/shard_map/reduce_scatter | solution.py:226
  274.6 93.6 %collective-permute-start = (bf16[2,2048]{1,0:T(2,128)(2,1)S(1)}, bf16[2,2048]{1,0:T(2,128)(2,1)S(1)}, u32[]{:S(2)}, u32[]{:S(2)}) collective-permute-start(bf16[2,2048]{1,0:T(2,128)(2,1)S(1)} %slice.72), channel_id=1, source_target_pairs={{0,4},{4,8},{8,12},{12,16},{16,20},{20,24},{24,28},{1,5},{5,9},{9,... | collective-permute-start | bytes 24584 | tf_op jit(solution)/shard_map/ppermute | solution.py:35
Sparse Core Ops, SparseCore 0:
  118.8 43.2 all-gather.21
  163.6 66.6 all-gather.11
  238.0 35.7 all-gather.13
  275.8 92.3 all-gather.15
  370.2 90.4 all-gather.17
  462.6 91.2 all-gather.19
  576.8 42.7 reduce-scatter.1
where the time goes:
time: 631 us; the launch traced here: 629 us
  waiting for transfers between devices  331 us (52%)
  local copies, waits for them, and re-layouts  97.1 us (15%)
  blocking collectives  84.7 us (13%)
  matrix products  67.5 us (11%)
  other arithmetic  29.4 us (5%)
  between operations  14.4 us (2%)
    all_gather x1, waiting for transfers between devices, local(): lax.all_gather(gate_up_weight, 'sp', axis=0, tiled=True)  90.1 us
    all_gather x1, waiting for transfers between devices, local(): lax.all_gather(down_projection_weight, 'sp', axis=1, tiled=True)  81.3 us
    all_gather x1, waiting for transfers between devices, local(): lax.all_gather(value_up_weight, 'sp', axis=0, tiled=True)  80.6 us
    dynamic_update_slice x16, local copies, waits for them, and re-layouts, local(): lax.scan(local_step, initial, (blocks(queries_low), blocks(keys_low), blo...  66.7 us
    reduce_scatter x1, waiting for transfers between devices, local(): lax.psum_scatter(jnp.dot(hidden, whole_down, preferred_element_type=jnp.f...  42.9 us
    all_gather x2, blocking collectives, carried_in(): lax.all_gather(part.astype(kind), axis)  40.3 us
    all_gather x1, waiting for transfers between devices, local(): group_rows = lax.all_gather(normed_rows, 'tp', axis=0, tiled=True)  33.9 us
    all_to_all x1, blocking collectives, local(): lax.all_to_all(gated_rows, 'tp', split_axis=0, concat_axis=1, tiled=True)  26.9 us
  transfers between devices with their start and end apart: 8, of which 5 were waited for; matrix products, arithmetic and copies ran while one was open for 8% of the time, Pallas kernels for 0%

commit v1 on v0

--- a/solution.py
+++ b/solution.py
@@ -222,7 +222,12 @@
         + value_filter_taps[2][None, :] * up_value[2:]
     )
     hidden = (jax.nn.silu(conv_g) * conv_v).astype(jnp.bfloat16)
-    whole_down = lax.all_gather(down_projection_weight, "sp", axis=1, tiled=True)
+    ring = [down_projection_weight]
+    for hop in range(7):
+        ring.append(lax.ppermute(ring[-1], "sp", [(dev, (dev + 1) % 8) for dev in range(8)]))
+    whole_down = jnp.roll(
+        jnp.concatenate(ring[::-1], axis=1), (lax.axis_index("sp") + 1) * ring[0].shape[1], axis=1
+    )
     ffn_rows = lax.psum_scatter(
         jnp.dot(hidden, whole_down, preferred_element_type=jnp.float32).astype(jnp.bfloat16),
         "tp",

time: 631 us -> 604 us (0.957)
  waiting for transfers between devices: 331 us -> 277 us
  local copies, waits for them, and re-layouts: 97.1 us -> 123 us
    ppermute x0 -> x7, waiting for transfers between devices: none -> 188 us  [local(): lax.ppermute(ring[-1], 'sp', [(dev, (dev + 1) % 8) for dev in range(8)])]
    all_gather x1 -> x0, waiting for transfers between devices: 81.3 us -> none  [local(): lax.all_gather(down_projection_weight, 'sp', axis=1, tiled=True)]
    all_gather x1, waiting for transfers between devices: 80.6 us -> 0.01 us  [local(): lax.all_gather(value_up_weight, 'sp', axis=0, tiled=True)]
    all_gather x1, waiting for transfers between devices: 90.1 us -> 43.6 us  [local(): lax.all_gather(gate_up_weight, 'sp', axis=0, tiled=True)]
    all_gather x1, waiting for transfers between devices: 33.9 us -> 0.01 us  [local(): group_rows = lax.all_gather(normed_rows, 'tp', axis=0, tiled=True)]
    unnamed x21 -> x48, local copies, waits for them, and re-layouts: 0.89 us -> 24.9 us
  transfers between devices with their start and end apart: 8 -> 14, of which waited for: 5 -> 11; matrix products, arithmetic and copies ran while one was open for 8% -> 10% of each run, Pallas kernels for 0% -> 0%
where the time goes in v1:
time: 604 us; the launch traced here: 602 us
  waiting for transfers between devices  277 us (46%)
  local copies, waits for them, and re-layouts  123 us (20%)
  blocking collectives  85.1 us (14%)
  matrix products  68.5 us (11%)
  other arithmetic  29.2 us (5%)
  between operations  14.3 us (2%)
    ppermute x7, waiting for transfers between devices, local(): lax.ppermute(ring[-1], 'sp', [(dev, (dev + 1) % 8) for dev in range(8)])  188 us
    dynamic_update_slice x16, local copies, waits for them, and re-layouts, local(): lax.scan(local_step, initial, (blocks(queries_low), blocks(keys_low), blo...  66.7 us
    all_gather x1, waiting for transfers between devices, local(): lax.all_gather(gate_up_weight, 'sp', axis=0, tiled=True)  43.6 us
    reduce_scatter x1, waiting for transfers between devices, local(): lax.psum_scatter(jnp.dot(hidden, whole_down, preferred_element_type=jnp.f...  42.9 us
    all_gather x2, blocking collectives, carried_in(): lax.all_gather(part.astype(kind), axis)  40.3 us
    all_to_all x1, blocking collectives, local(): lax.all_to_all(gated_rows, 'tp', split_axis=0, concat_axis=1, tiled=True)  27.3 us
    unnamed x48, local copies, waits for them, and re-layouts  24.9 us
    dot_general x1, matrix products, local(): jnp.dot(hidden, whole_down, preferred_element_type=jnp.float32)  23.7 us
  transfers between devices with their start and end apart: 14, of which 11 were waited for; matrix products, arithmetic and copies ran while one was open for 10% of the time, Pallas kernels for 0%

profile of v1, /device:TPU:0, one launch (start us, length us, event | category | flops | bytes accessed | tf_op | source)
XLA Modules:
  0.0 601.8 jit_solution(10842242744348345828)
XLA Ops:
  8.5 1.3 reshape.215
  9.8 2.0 reshape.216
  11.8 2.0 reshape.217
  13.8 105.1 %while.39 = (s32[]{:T(128)}, f32[2,256,128]{2,1,0:T(8,128)S(1)}, f32[2,128]{1,0:T(2,128)S(1)}, f32[2]{0:T(128)S(1)}, f32[8,128,2,256]{1,0,3,2:T(8,128)}, /*index...) while((s32[]{:T(128)}, f32[2,256,128]{2,1,0:T(8,128)S(1)}, ...), condition=%wide.region_6.7_spmd.clone, body=%wide.region_0.6_spmd.clone.sunk | while | flops 144166400 | bytes 4685110 | solution.py:144
  18.7 8.2 %dynamic_update_slice.19 = f32[8,128,2,256]{1,0,3,2:T(8,128)} dynamic-update-slice(f32[8,128,2,256]{1,0,3,2:T(8,128)} %get-tuple-element.661, f32[1,128,2,256]{1,0,3,2:T(1,128)S(1)} %copy.248, s32[]{:T(128)S(6)} %copy.260, s32[]{:T(128)} %constant.103.clone.1..sunk, s32[]{:T(128)} %constant.103.clone.1..sunk, s32[]{:T(128)} %constant.103.clone.1..sunk) | dynamic-update-slice | bytes 524292 | tf_op jit(solution)/shard_map/while/body/jit(dynamic_update_index_in_dim)/dynamic_update_slice | solution.py:144
  31.8 8.2 %dynamic_update_slice.19 = f32[8,128,2,256]{1,0,3,2:T(8,128)} dynamic-update-slice(f32[8,128,2,256]{1,0,3,2:T(8,128)} %get-tuple-element.661, f32[1,128,2,256]{1,0,3,2:T(1,128)S(1)} %copy.248, s32[]{:T(128)S(6)} %copy.260, s32[]{:T(128)} %constant.103.clone.1..sunk, s32[]{:T(128)} %constant.103.clone.1..sunk, s32[]{:T(128)} %constant.103.clone.1..sunk) | dynamic-update-slice | bytes 524292 | tf_op jit(solution)/shard_map/while/body/jit(dynamic_update_index_in_dim)/dynamic_update_slice | solution.py:144
  45.0 8.2 %dynamic_update_slice.19 = f32[8,128,2,256]{1,0,3,2:T(8,128)} dynamic-update-slice(f32[8,128,2,256]{1,0,3,2:T(8,128)} %get-tuple-element.661, f32[1,128,2,256]{1,0,3,2:T(1,128)S(1)} %copy.248, s32[]{:T(128)S(6)} %copy.260, s32[]{:T(128)} %constant.103.clone.1..sunk, s32[]{:T(128)} %constant.103.clone.1..sunk, s32[]{:T(128)} %constant.103.clone.1..sunk) | dynamic-update-slice | bytes 524292 | tf_op jit(solution)/shard_map/while/body/jit(dynamic_update_index_in_dim)/dynamic_update_slice | solution.py:144
  58.1 8.2 %dynamic_update_slice.19 = f32[8,128,2,256]{1,0,3,2:T(8,128)} dynamic-update-slice(f32[8,128,2,256]{1,0,3,2:T(8,128)} %get-tuple-element.661, f32[1,128,2,256]{1,0,3,2:T(1,128)S(1)} %copy.248, s32[]{:T(128)S(6)} %copy.260, s32[]{:T(128)} %constant.103.clone.1..sunk, s32[]{:T(128)} %constant.103.clone.1..sunk, s32[]{:T(128)} %constant.103.clone.1..sunk) | dynamic-update-slice | bytes 524292 | tf_op jit(solution)/shard_map/while/body/jit(dynamic_update_index_in_dim)/dynamic_update_slice | solution.py:144
  71.3 8.2 %dynamic_update_slice.19 = f32[8,128,2,256]{1,0,3,2:T(8,128)} dynamic-update-slice(f32[8,128,2,256]{1,0,3,2:T(8,128)} %get-tuple-element.661, f32[1,128,2,256]{1,0,3,2:T(1,128)S(1)} %copy.248, s32[]{:T(128)S(6)} %copy.260, s32[]{:T(128)} %constant.103.clone.1..sunk, s32[]{:T(128)} %constant.103.clone.1..sunk, s32[]{:T(128)} %constant.103.clone.1..sunk) | dynamic-update-slice | bytes 524292 | tf_op jit(solution)/shard_map/while/body/jit(dynamic_update_index_in_dim)/dynamic_update_slice | solution.py:144
  84.4 8.2 %dynamic_update_slice.19 = f32[8,128,2,256]{1,0,3,2:T(8,128)} dynamic-update-slice(f32[8,128,2,256]{1,0,3,2:T(8,128)} %get-tuple-element.661, f32[1,128,2,256]{1,0,3,2:T(1,128)S(1)} %copy.248, s32[]{:T(128)S(6)} %copy.260, s32[]{:T(128)} %constant.103.clone.1..sunk, s32[]{:T(128)} %constant.103.clone.1..sunk, s32[]{:T(128)} %constant.103.clone.1..sunk) | dynamic-update-slice | bytes 524292 | tf_op jit(solution)/shard_map/while/body/jit(dynamic_update_index_in_dim)/dynamic_update_slice | solution.py:144
  97.5 8.2 %dynamic_update_slice.19 = f32[8,128,2,256]{1,0,3,2:T(8,128)} dynamic-update-slice(f32[8,128,2,256]{1,0,3,2:T(8,128)} %get-tuple-element.661, f32[1,128,2,256]{1,0,3,2:T(1,128)S(1)} %copy.248, s32[]{:T(128)S(6)} %copy.260, s32[]{:T(128)} %constant.103.clone.1..sunk, s32[]{:T(128)} %constant.103.clone.1..sunk, s32[]{:T(128)} %constant.103.clone.1..sunk) | dynamic-update-slice | bytes 524292 | tf_op jit(solution)/shard_map/while/body/jit(dynamic_update_index_in_dim)/dynamic_update_slice | solution.py:144
  110.7 8.2 %dynamic_update_slice.19 = f32[8,128,2,256]{1,0,3,2:T(8,128)} dynamic-update-slice(f32[8,128,2,256]{1,0,3,2:T(8,128)} %get-tuple-element.661, f32[1,128,2,256]{1,0,3,2:T(1,128)S(1)} %copy.248, s32[]{:T(128)S(6)} %copy.260, s32[]{:T(128)} %constant.103.clone.1..sunk, s32[]{:T(128)} %constant.103.clone.1..sunk, s32[]{:T(128)} %constant.103.clone.1..sunk) | dynamic-update-slice | bytes 524292 | tf_op jit(solution)/shard_map/while/body/jit(dynamic_update_index_in_dim)/dynamic_update_slice | solution.py:144
  123.1 22.3 %all-gather.3 = bf16[8,1,2]{2,1,0:T(2,128)(2,1)S(1)} all-gather(bf16[1,1,2]{2,1,0:T(2,128)(2,1)S(1)} %bitcast.274), channel_id=1, replica_groups=mesh['sp'=8,'tp'=4] {'sp'}, dimensions={0}, use_global_device_ids=true | all-gather | bytes 36 | tf_op jit(solution)/shard_map/all_gather | solution.py:14
  145.4 17.5 %all-reduce = bf16[16]{0:T(256)(128)(2,1)S(1)} all-reduce(bf16[16]{0:T(256)(128)(2,1)S(1)} %dynamic-update-slice), channel_id=2, replica_groups=mesh['sp'=8,'tp'=4] {'sp'}, use_global_device_ids=true, to_apply=%add | all-reduce | flops 16 | bytes 64
  163.0 1.2 copy.155
  164.4 1.3 copy.156
  165.6 1.7 reshape.187
  167.3 18.0 %all-gather.4 = bf16[8,2,128]{2,1,0:T(2,128)(2,1)S(1)} all-gather(bf16[1,2,128]{2,1,0:T(2,128)(2,1)S(1)} %convert_bitcast_fusion), channel_id=4, replica_groups=mesh['sp'=8,'tp'=4] {'sp'}, dimensions={0}, use_global_device_ids=true | all-gather | bytes 4608 | tf_op jit(solution)/shard_map/all_gather | solution.py:14
  185.4 10.5 %while.40 = (s32[]{:T(128)}, f32[2,256,128]{2,1,0:T(8,128)S(1)}, f32[2,128]{1,0:T(2,128)S(1)}, f32[2]{0:T(128)S(1)}, s32[]{:T(128)}, /*index=5*/bf16[8,2]{0,1:T(...) while((s32[]{:T(128)}, f32[2,256,128]{2,1,0:T(8,128)S(1)}, ...), condition=%wide.region_10.11_spmd.clone, body=%wide.region_9.10_spmd.clone.sunk | while | flops 394772 | bytes 658165 | solution.py:29
  186.9 1.0 fusion.112
  195.9 1.0 fusion.57
  197.0 2.2 multiply_reduce_fusion
  199.5 1.9 copy.141
  201.4 2.1 multiply_convert_fusion
  203.6 27.3 %all_to_all.19 = bf16[4,256,512]{2,1,0:T(8,128)(2,1)S(1)} all-to-all(bf16[4,256,512]{2,1,0:T(8,128)(2,1)S(1)} %bitcast.261), channel_id=1, replica_groups=mesh['sp'=8,'tp'=4] {'tp'}, dimensions={0} | all-to-all | bytes 2097152 | tf_op jit(solution)/shard_map/all_to_all | solution.py:191
  231.8 6.0 %fusion.50 = bf16[256,2048]{1,0:T(8,128)(2,1)S(1)} fusion(bf16[256,2048]{0,1:T(8,128)(2,1)S(1)} %bitcast.259, bf16[2048,2048]{1,0:T(8,128)(2,1)} %all-gather.11.cloned.1.call-done, bf16[256,2048]{1,0:T(8,128)(2,1)} %param.20), kind=kOutput, calls=%fused_computation.94 | convolution fusion | flops 2149056512 | bytes 11534336 | tf_op jit(solution)/shard_map/dot_general | solution.py:192
  238.1 1.3 fusion.53
  240.0 2.4 collective-permute-start.1
  242.5 19.3 %collective-permute-done.1 = bf16[1408,256]{1,0:T(8,128)(2,1)S(1)} collective-permute-done((bf16[1408,256]{1,0:T(8,128)(2,1)S(1)}, bf16[1408,256]{1,0:T(8,128)(2,1)S(1)}, u32[]{:S(2)}, u32[]{:S(2)}) %collective-permute-start.1) | collective-permute-done | bytes 720928 | tf_op jit(solution)/shard_map/ppermute | solution.py:227
  261.8 20.3 %collective-permute-done.2 = bf16[1408,256]{1,0:T(8,128)(2,1)S(1)} collective-permute-done((bf16[1408,256]{1,0:T(8,128)(2,1)S(1)}, bf16[1408,256]{1,0:T(8,128)(2,1)S(1)}, u32[]{:S(2)}, u32[]{:S(2)}) %collective-permute-start.2) | collective-permute-done | bytes 720928 | tf_op jit(solution)/shard_map/ppermute | solution.py:227
  282.2 32.6 %collective-permute-done.3 = bf16[1408,256]{1,0:T(8,128)(2,1)S(1)} collective-permute-done((bf16[1408,256]{1,0:T(8,128)(2,1)S(1)}, bf16[1408,256]{1,0:T(8,128)(2,1)S(1)}, u32[]{:S(2)}, u32[]{:S(2)}) %collective-permute-start.3) | collective-permute-done | bytes 720928 | tf_op jit(solution)/shard_map/ppermute | solution.py:227
  315.6 24.8 %collective-permute-done.4 = bf16[1408,256]{1,0:T(8,128)(2,1)S(1)} collective-permute-done((bf16[1408,256]{1,0:T(8,128)(2,1)S(1)}, bf16[1408,256]{1,0:T(8,128)(2,1)S(1)}, u32[]{:S(2)}, u32[]{:S(2)}) %collective-permute-start.4) | collective-permute-done | bytes 720928 | tf_op jit(solution)/shard_map/ppermute | solution.py:227
  341.3 36.1 %collective-permute-done.5 = bf16[1408,256]{1,0:T(8,128)(2,1)S(1)} collective-permute-done((bf16[1408,256]{1,0:T(8,128)(2,1)S(1)}, bf16[1408,256]{1,0:T(8,128)(2,1)S(1)}, u32[]{:S(2)}, u32[]{:S(2)}) %collective-permute-start.5) | collective-permute-done | bytes 720928 | tf_op jit(solution)/shard_map/ppermute | solution.py:227
  378.3 34.1 %collective-permute-done.6 = bf16[1408,256]{1,0:T(8,128)(2,1)} collective-permute-done((bf16[1408,256]{1,0:T(8,128)(2,1)S(1)}, bf16[1408,256]{1,0:T(8,128)(2,1)}, u32[]{:S(2)}, u32[]{:S(2)}) %collective-permute-start.6) | collective-permute-done | bytes 720928 | tf_op jit(solution)/shard_map/ppermute | solution.py:227
  412.5 21.2 %collective-permute-done.7 = bf16[1408,256]{1,0:T(8,128)(2,1)} collective-permute-done((bf16[1408,256]{1,0:T(8,128)(2,1)}, bf16[1408,256]{1,0:T(8,128)(2,1)}, u32[]{:S(2)}, u32[]{:S(2)}) %collective-permute-start.7) | collective-permute-done | bytes 720928 | tf_op jit(solution)/shard_map/ppermute | solution.py:227
  433.7 2.1 constant_dynamic-update-slice_fusion.15
  435.8 2.1 constant_dynamic-update-slice_fusion.14
  437.9 2.2 constant_dynamic-update-slice_fusion.13
  440.1 2.2 constant_dynamic-update-slice_fusion.12
  446.1 2.1 constant_dynamic-update-slice_fusion.7
  448.2 2.1 constant_dynamic-update-slice_fusion.6
  455.9 1.3 collective-permute-start
  458.6 11.8 %fusion.48 = f32[1026,1408]{1,0:T(8,128)} fusion(bf16[2048,1408]{1,0:T(8,128)(2,1)} %all-gather.17.cloned.1.call-done, bf16[1024,2048]{1,0:T(8,128)(2,1)} %all-gather.13.cloned.1.call-done, bf16[2,2048]{1,0:T(2,128)(2,1)S(1)} %collective-permute-done), kind=kOutput, calls=%fused_computation.91 | convolution fusion | flops 5925519360 | bytes 15748096 | tf_op jit(solution)/shard_map/dot_general | solution.py:209
  470.4 43.6 %all-gather.15.cloned.1.call-done = bf16[2048,1408]{1,0:T(8,128)(2,1)} async-done(((bf16[256,1408]{1,0:T(8,128)(2,1)}), bf16[2048,1408]{1,0:T(8,128)(2,1)}) %all-gather.15.cloned.1.call-update) | async-done | bytes 5767184 | tf_op jit(solution)/shard_map/all_gather | solution.py:206
  513.9 11.8 %fusion.49 = f32[1026,1408]{1,0:T(8,128)} fusion(bf16[2048,1408]{1,0:T(8,128)(2,1)} %all-gather.15.cloned.1.call-done, bf16[1024,2048]{1,0:T(8,128)(2,1)} %all-gather.13.cloned.1.call-done, bf16[2,2048]{1,0:T(2,128)(2,1)S(1)} %collective-permute-done), kind=kOutput, calls=%fused_computation.92 | convolution fusion | flops 5925519360 | bytes 15748096 | tf_op jit(solution)/shard_map/dot_general | solution.py:204
  525.8 23.7 %fusion.44 = bf16[1024,2048]{1,0:T(8,128)(2,1)} fusion(bf16[1408,4096]{1,0:T(8,128)(2,1)} %constant_dynamic-update-slice_fusion, s32[]{:T(128)S(6)} %select_n.82, f32[1026,1408]{1,0:T(8,128)} %fusion.48, f32[1026,1408]{1,0:T(8,128)} %fusion.49, f32[1408]{0:T(1024)S(1)} %get-tuple-element.403, f32[1408]{0:T(1024)S(1)} %get-tuple-element.404, ...), kind=kOutput, calls=%fused_computation.87 | convolution fusion | flops 5930745856 | bytes 44598276 | tf_op jit(solution)/shard_map/dot_general | solution.py:232
  549.5 42.9 %reduce-scatter.2.cloned.1.call-done = bf16[256,2048]{1,0:T(8,128)(2,1)} async-done(((bf16[1024,2048]{1,0:T(8,128)(2,1)}), bf16[256,2048]{1,0:T(8,128)(2,1)}) %reduce-scatter.2.cloned.1.call-update) | async-done | bytes 1048592 | tf_op jit(solution)/shard_map/reduce_scatter | solution.py:231
  592.4 2.6 fusion.54
  (360 shorter events, 69.5 us)
Async XLA Ops:
  6.5 178.8 %all-gather.19.cloned.1.call-start = ((), (), s32[]{:S(2)}) async-start(), calls=%async_computation.7 | async-start | bytes 1179648 | tf_op jit(solution)/shard_map/all_gather | solution.py:14
  13.8 107.7 %copy-start.13 = (u32[32]{0:T(128)S(1)}, u32[32]{0:T(128)}, u32[]{:S(2)}) copy-start(u32[32]{0:T(128)} %constant.126) | copy-start | bytes 388
  118.9 77.0 %copy-start.8 = (bf16[1024,256]{1,0:T(8,128)(2,1)S(1)}, bf16[1024,256]{1,0:T(8,128)(2,1)}, u32[]{:S(2)}) copy-start(bf16[1024,256]{1,0:T(8,128)(2,1)} %param.21) | copy-start | bytes 1572868
  119.6 112.2 %all-gather.11.cloned.1.call-start = ((), (), s32[]{:S(2)}) async-start(), calls=%async_computation.2 | async-start | bytes 10485760 | tf_op jit(solution)/shard_map/all_gather | solution.py:190
  120.3 334.8 %all-gather.13.cloned.1.call-start = ((), (), s32[]{:S(2)}) async-start(), calls=%async_computation.3 | async-start | bytes 5242880 | tf_op jit(solution)/shard_map/all_gather | solution.py:201
  195.9 3.4 copy-start.12
  199.2 2.2 copy-start.7
  231.8 6.3 %copy-start.11 = (f32[2048]{0:T(1024)S(1)}, f32[2048]{0:T(1024)}, u32[]{:S(2)}) copy-start(f32[2048]{0:T(1024)} %param.30) | copy-start | bytes 24580
  231.8 8.3 %copy-start = (bf16[1408,256]{1,0:T(8,128)(2,1)S(1)}, bf16[1408,256]{1,0:T(8,128)(2,1)}, u32[]{:S(2)}) copy-start(bf16[1408,256]{1,0:T(8,128)(2,1)} %param.35) | copy-start | bytes 2162692
  231.8 180.6 %copy-start.9 = (f32[3,1408]{1,0:T(4,128)S(1)}, f32[3,1408]{1,0:T(4,128)}, u32[]{:S(2)}) copy-start(f32[3,1408]{1,0:T(4,128)} %param.34) | copy-start | bytes 50692
  231.8 180.6 %copy-start.10 = (f32[3,1408]{1,0:T(4,128)S(1)}, f32[3,1408]{1,0:T(4,128)}, u32[]{:S(2)}) copy-start(f32[3,1408]{1,0:T(4,128)} %param.33) | copy-start | bytes 50692
  239.4 218.8 %all-gather.17.cloned.1.call-start = ((), (), s32[]{:S(2)}) async-start(), calls=%async_computation.5 | async-start | bytes 6488064 | tf_op jit(solution)/shard_map/all_gather | solution.py:211
  240.0 273.9 %all-gather.15.cloned.1.call-start = ((), (), s32[]{:S(2)}) async-start(), calls=%async_computation.4 | async-start | bytes 6488064 | tf_op jit(solution)/shard_map/all_gather | solution.py:206
  240.0 21.7 %collective-permute-start.1 = (bf16[1408,256]{1,0:T(8,128)(2,1)S(1)}, bf16[1408,256]{1,0:T(8,128)(2,1)S(1)}, u32[]{:S(2)}, u32[]{:S(2)}) collective-permute-start(bf16[1408,256]{1,0:T(8,128)(2,1)S(1)} %copy-done), channel_id=1, source_target_pairs={{0,4},{4,8},{8,12},{12,16},{16,20},{20,24},{24,28},{28,0},{1,5},{5... | collective-permute-start | bytes 2162696 | tf_op jit(solution)/shard_map/ppermute | solution.py:227
  261.8 20.4 %collective-permute-start.2 = (bf16[1408,256]{1,0:T(8,128)(2,1)S(1)}, bf16[1408,256]{1,0:T(8,128)(2,1)S(1)}, u32[]{:S(2)}, u32[]{:S(2)}) collective-permute-start(bf16[1408,256]{1,0:T(8,128)(2,1)S(1)} %collective-permute-done.1), channel_id=1, source_target_pairs={{0,4},{4,8},{8,12},{12,16},{16,20},{20,24},{24,28},{28,0},{1,5},{5... | collective-permute-start | bytes 2162696 | tf_op jit(solution)/shard_map/ppermute | solution.py:227
  261.8 330.6 %reduce-scatter.2.cloned.1.call-start = ((), (), s32[]{:S(2)}) async-start(), calls=%async_computation.6 | async-start | bytes 5242880 | tf_op jit(solution)/shard_map/reduce_scatter | solution.py:231
  282.2 32.6 %collective-permute-start.3 = (bf16[1408,256]{1,0:T(8,128)(2,1)S(1)}, bf16[1408,256]{1,0:T(8,128)(2,1)S(1)}, u32[]{:S(2)}, u32[]{:S(2)}) collective-permute-start(bf16[1408,256]{1,0:T(8,128)(2,1)S(1)} %collective-permute-done.2), channel_id=1, source_target_pairs={{0,4},{4,8},{8,12},{12,16},{16,20},{20,24},{24,28},{28,0},{1,5},{5... | collective-permute-start | bytes 2162696 | tf_op jit(solution)/shard_map/ppermute | solution.py:227
  314.8 0.9 copy-start.1
  315.6 24.8 %collective-permute-start.4 = (bf16[1408,256]{1,0:T(8,128)(2,1)S(1)}, bf16[1408,256]{1,0:T(8,128)(2,1)S(1)}, u32[]{:S(2)}, u32[]{:S(2)}) collective-permute-start(bf16[1408,256]{1,0:T(8,128)(2,1)S(1)} %collective-permute-done.3), channel_id=1, source_target_pairs={{0,4},{4,8},{8,12},{12,16},{16,20},{20,24},{24,28},{28,0},{1,5},{5... | collective-permute-start | bytes 2162696 | tf_op jit(solution)/shard_map/ppermute | solution.py:227
  340.4 0.9 copy-start.3
  341.3 36.1 %collective-permute-start.5 = (bf16[1408,256]{1,0:T(8,128)(2,1)S(1)}, bf16[1408,256]{1,0:T(8,128)(2,1)S(1)}, u32[]{:S(2)}, u32[]{:S(2)}) collective-permute-start(bf16[1408,256]{1,0:T(8,128)(2,1)S(1)} %collective-permute-done.4), channel_id=1, source_target_pairs={{0,4},{4,8},{8,12},{12,16},{16,20},{20,24},{24,28},{28,0},{1,5},{5... | collective-permute-start | bytes 2162696 | tf_op jit(solution)/shard_map/ppermute | solution.py:227
  377.4 0.9 copy-start.5
  378.3 34.1 %collective-permute-start.6 = (bf16[1408,256]{1,0:T(8,128)(2,1)S(1)}, bf16[1408,256]{1,0:T(8,128)(2,1)}, u32[]{:S(2)}, u32[]{:S(2)}) collective-permute-start(bf16[1408,256]{1,0:T(8,128)(2,1)S(1)} %collective-permute-done.5), channel_id=1, source_target_pairs={{0,4},{4,8},{8,12},{12,16},{16,20},{20,24},{24,28},{28,0},{1,5},{5... | collective-permute-start | bytes 2162696 | tf_op jit(solution)/shard_map/ppermute | solution.py:227
  412.4 21.3 %collective-permute-start.7 = (bf16[1408,256]{1,0:T(8,128)(2,1)}, bf16[1408,256]{1,0:T(8,128)(2,1)}, u32[]{:S(2)}, u32[]{:S(2)}) collective-permute-start(bf16[1408,256]{1,0:T(8,128)(2,1)} %collective-permute-done.6), channel_id=1, source_target_pairs={{0,4},{4,8},{8,12},{12,16},{16,20},{20,24},{24,28},{28,0},{1,5},{5... | collective-permute-start | bytes 2162696 | tf_op jit(solution)/shard_map/ppermute | solution.py:227
  412.4 29.9 %copy-start.2 = (bf16[1408,256]{1,0:T(8,128)(2,1)S(1)}, bf16[1408,256]{1,0:T(8,128)(2,1)}, u32[]{:S(2)}) copy-start(bf16[1408,256]{1,0:T(8,128)(2,1)} %copy-done.1) | copy-start | bytes 2162692
  437.9 12.4 %copy-start.6 = (bf16[1408,256]{1,0:T(8,128)(2,1)S(1)}, bf16[1408,256]{1,0:T(8,128)(2,1)}, u32[]{:S(2)}) copy-start(bf16[1408,256]{1,0:T(8,128)(2,1)} %copy-done.5) | copy-start | bytes 2162692
  440.1 11.2 %copy-start.4 = (bf16[1408,256]{1,0:T(8,128)(2,1)S(1)}, bf16[1408,256]{1,0:T(8,128)(2,1)}, u32[]{:S(2)}) copy-start(bf16[1408,256]{1,0:T(8,128)(2,1)} %copy-done.3) | copy-start | bytes 2162692
  455.9 2.6 collective-permute-start
Sparse Core Ops, SparseCore 0:
  119.7 43.2 all-gather.18
  164.5 67.1 all-gather.10
  239.5 35.3 all-gather.12
  276.9 133.1 all-gather.16
  412.2 101.6 all-gather.14
  549.6 42.7 reduce-scatter.1
